TPU v7x, 256 devices: a 4x2x16 block of a 4x16x16 slice. The times are simulated.
256 devices in a mesh: grp: 2 (over y), kv: 16 (over z), tp: 8 (over x, core).
Axes of the slice: x: 4, y: 2, z: 16, core: 2. Of those that a mesh axis runs over, the one named last changes fastest.
The devices are a block of a 4x16x16 slice.
Arguments:
- tokens: bfloat16 [16, 4096], P('grp', ('kv', 'tp')), parts along dimension 0, may hold values from -16 to 16
- key_cache: bfloat16 [16, 8192, 8, 256], P('grp', 'kv', 'tp'), parts along dimension 0, may hold values from -1200 to 1200
- value_cache: bfloat16 [16, 8192, 8, 256], P('grp', 'kv', 'tp'), parts along dimension 0, may hold values from -6 to 6
- gain_first: float32 [4096], replicated, may hold values from 0.1 to 1.9
- gate_first: bfloat16 [4096, 11008], P(None, ('kv', 'tp')), may hold values from -0.09375 to 0.09375
- up_first: bfloat16 [4096, 11008], P(None, ('kv', 'tp')), may hold values from -0.09375 to 0.09375
- down_first: bfloat16 [11008, 4096], P(('kv', 'tp')), may hold values from -0.0546875 to 0.0546875
- gain_mix: float32 [4096], replicated, may hold values from 0.1 to 1.9
- query_first: bfloat16 [4096, 1024], P('kv', 'tp'), may hold values from -0.09375 to 0.09375
- query_second: bfloat16 [4096, 1024], P('kv', 'tp'), may hold values from -0.09375 to 0.09375
- key_first: bfloat16 [4096, 1024], P('kv', 'tp'), may hold values from -0.5 to 0.5
- key_second: bfloat16 [4096, 1024], P('kv', 'tp'), may hold values from -0.5 to 0.5
- value_weight: bfloat16 [4096, 2048], P('kv', 'tp'), may hold values from -0.09375 to 0.09375
- mix_lambda: float32 [8], P('tp'), may hold values from 0.3 to 0.8
- head_gain: float32 [8, 256], P('tp'), may hold values from 0.1 to 1.9
- out_weight: bfloat16 [2048, 4096], P('tp', 'kv'), may hold values from -0.125 to 0.125
- gain_last: float32 [4096], replicated, may hold values from 0.1 to 1.9
- gate_last: bfloat16 [4096, 11008], P(None, ('kv', 'tp')), may hold values from -0.09375 to 0.09375
- up_last: bfloat16 [4096, 11008], P(None, ('kv', 'tp')), may hold values from -0.09375 to 0.09375
- down_last: bfloat16 [11008, 4096], P(('kv', 'tp')), may hold values from -0.0546875 to 0.0546875
Outputs:
- updated: bfloat16 [16, 4096], P('grp', ('kv', 'tp')), parts along dimension 0
There are 2 independent parts, one for each index of `grp`. A program takes and returns all parts, laid end to end along the dimension named above; an argument that names none is the same for every part. Nothing has to cross between parts.
All inputs are finite; a program needn't handle non-finite values.
Results may differ from a plain program's by a relative error of at most 0.02.
Values may be sent and summed in bfloat16 or wider, within the bound.
A program may use at most 64 MiB of HBM per device.

v0:
```python
import jax
import jax.numpy as jnp
from jax import lax
from jax.sharding import Mesh
from jax.sharding import PartitionSpec as P

KV_TP = ("kv", "tp_0", "tp_1")
TP = ("tp_0", "tp_1")


norm_eps = 1e-06


def laid_out(pieces, dim):
    dims = list(pieces.shape[1:])
    dims[dim] *= pieces.shape[0]
    return jnp.moveaxis(pieces, 0, dim).reshape(dims)


def gather_in_order(shard, axes, order):
    pieces = shard
    for k in order:
        pieces = lax.all_gather(pieces, axes[k])
    done = order[::-1]
    back = [done.index(k) for k in range(len(axes))]
    pieces = pieces.transpose(*back, *range(len(axes), pieces.ndim))
    return pieces.reshape(-1, *shard.shape)


def gather_axes(shard, axes, order, dim):
    return laid_out(gather_in_order(shard, axes, order), dim)


def reduced_to_own(pieces, axes, order):
    dims = [lax.axis_size(a) for a in axes]
    pieces = pieces.reshape(*dims, *pieces.shape[1:])
    pieces = pieces.transpose(*order, *range(len(axes), pieces.ndim))
    pieces = pieces.reshape(-1, *pieces.shape[len(axes) :])
    for k in order:
        pieces = lax.psum_scatter(pieces, axes[k], scatter_dimension=0, tiled=True)
    return pieces[0]


def cut_along(shard, dim, count):
    before, after = (shard.shape[:dim], shard.shape[dim + 1 :])
    return jnp.moveaxis(shard.reshape(*before, count, -1, *after), dim, 0)


def sum_by_axis(shard, axes, order, dim):
    count = lax.axis_size(axes)
    return reduced_to_own(cut_along(shard, dim, count), axes, order)


def copy_for_each(shard, axis):
    count = lax.axis_size(axis)
    return lax.all_to_all(
        jnp.broadcast_to(shard[None], (count, *shard.shape)), axis, 0, 0, tiled=True
    )


def of_everyone(shard, axis):
    return copy_for_each(shard, axis).sum(axis=0)


def in_one(arrays, axis):
    flat, at, outs = (jnp.concatenate([a.reshape(-1) for a in arrays]), 0, [])
    so_far = of_everyone(flat, axis)
    for a in arrays:
        outs.append(so_far[at : at + a.size].reshape(a.shape))
        at += a.size
    return tuple(outs)


def all_in_one(shard, axis):
    leaves = jax.tree.leaves(shard)
    order = sorted(range(len(leaves)), key=lambda k: -leaves[k].size)
    width = (1, *leaves[order[0]].shape)[-1]
    lines = [
        jnp.pad(leaves[k].reshape(-1), (0, -leaves[k].size % width)).reshape(-1, width)
        for k in order
    ]
    both, at, found = (copy_for_each(jnp.concatenate(lines), axis), 0, {})
    for k, line in zip(order, lines):
        piece = both[:, at : at + len(line)].reshape(len(both), -1)
        found[k] = piece[:, : leaves[k].size].reshape(-1, *leaves[k].shape)
        at += len(line)
    numbers = iter(range(len(leaves)))
    return jax.tree.map(lambda _: found[next(numbers)], shard)


def joined_by_halves(pieces, combine):
    while len(jax.tree.leaves(pieces)[0]) > 1:
        pieces = jax.vmap(combine)(
            *(jax.tree.map(lambda part: part[side::2], pieces) for side in (0, 1))
        )
    return jax.tree.map(lambda part: part[0], pieces)


def merged_2(shard, axis, combine):
    pieces = all_in_one(shard, axis)
    return joined_by_halves(pieces, combine)


def summed_on_arrival(shard, axis, dim):
    pieces = cut_along(shard, dim, lax.axis_size(axis))
    arrived = lax.all_to_all(pieces, axis, split_axis=0, concat_axis=0, tiled=True)
    return arrived.astype(jnp.float32).sum(axis=0)


def hidden_units(whole_rows, gain_vec, weight_gate, weight_up):
    wide_rows = whole_rows.astype(jnp.float32)
    row_factor = lax.rsqrt(jnp.mean(wide_rows * wide_rows, axis=-1, keepdims=True) + norm_eps)
    normed = (wide_rows * gain_vec).astype(jnp.bfloat16)
    gate_value = row_factor * jnp.dot(normed, weight_gate, preferred_element_type=jnp.float32)
    up_value = row_factor * jnp.dot(normed, weight_up, preferred_element_type=jnp.float32)
    return (jax.nn.silu(gate_value) * up_value).astype(jnp.bfloat16)


def down_term(hidden, weight_down):
    return lax.dot_general(
        weight_down, hidden, (((0,), (1,)), ((), ())), preferred_element_type=jnp.float32
    )


def block_softmax(queries, key_block, value_block, head_dim):
    scores = jnp.einsum(
        "bhd,bphd->bhp", queries, key_block, preferred_element_type=jnp.float32
    ) * head_dim ** (-0.5)
    top_score = jnp.max(scores, axis=-1)
    weights = jnp.exp(scores - top_score[..., None])
    weight_sum = jnp.sum(weights, axis=-1)
    weighted = jnp.einsum(
        "bhp,bphd->bhd",
        weights.astype(jnp.bfloat16),
        value_block,
        preferred_element_type=jnp.float32,
    )
    return (top_score, weight_sum, weighted)


def combine_maps(earlier, later):
    merged = ()
    for offset in (0, 3):
        top_a, total_a, accum_a = (earlier[offset], earlier[offset + 1], earlier[offset + 2])
        top_b, total_b, accum_b = (later[offset], later[offset + 1], later[offset + 2])
        top_new = jnp.maximum(top_a, top_b)
        factor_a = jnp.exp(top_a - top_new)
        factor_b = jnp.exp(top_b - top_new)
        merged = merged + (
            top_new,
            factor_a * total_a + factor_b * total_b,
            factor_a[..., None] * accum_a + factor_b[..., None] * accum_b,
        )
    return merged


def with_own(stats, own_score, own_value):
    top_score, weight_sum, weighted = stats
    top_new = jnp.maximum(top_score, own_score)
    factor_old = jnp.exp(top_score - top_new)
    factor_own = jnp.exp(own_score - top_new)
    total_sum = factor_old * weight_sum + factor_own
    accum_sum = factor_old[..., None] * weighted + factor_own[..., None] * own_value.astype(
        jnp.float32
    )
    return accum_sum / total_sum[..., None]


def local(
    tokens,
    key_cache,
    value_cache,
    gain_first,
    gate_first,
    up_first,
    down_first,
    gain_mix,
    query_first,
    query_second,
    key_first,
    key_second,
    value_weight,
    mix_lambda,
    head_gain,
    out_weight,
    gain_last,
    gate_last,
    up_last,
    down_last,
):
    batch_rows, own_width = tokens.shape
    heads_here = mix_lambda.shape[0]
    head_dim = query_first.shape[1] // heads_here
    entry_whole = gather_axes(tokens, KV_TP, (1, 0, 2), 1)
    hidden_one = hidden_units(entry_whole, gain_first, gate_first, up_first)
    mixed_own = sum_by_axis(down_term(hidden_one, down_first), KV_TP, (2, 0, 1), 0)
    stream_own = (tokens.astype(jnp.float32) + 0.5 * mixed_own.T).astype(jnp.bfloat16)
    stream_whole = gather_axes(stream_own, KV_TP, (1, 0, 2), 1)
    mix_rows = stream_whole.astype(jnp.float32)
    mix_factor = lax.rsqrt(jnp.mean(mix_rows * mix_rows, axis=-1, keepdims=True) + norm_eps)
    rows_here = query_first.shape[0]
    row_start = lax.axis_index("kv") * rows_here
    normed_part = (
        lax.dynamic_slice_in_dim(mix_rows, row_start, rows_here, 1)
        * lax.dynamic_slice_in_dim(gain_mix, row_start, rows_here, 0)
    ).astype(jnp.bfloat16)
    summed = in_one(
        (
            jnp.dot(normed_part, query_first, preferred_element_type=jnp.float32),
            jnp.dot(normed_part, query_second, preferred_element_type=jnp.float32),
            jnp.dot(normed_part, key_first, preferred_element_type=jnp.float32),
            jnp.dot(normed_part, key_second, preferred_element_type=jnp.float32),
            jnp.dot(normed_part, value_weight, preferred_element_type=jnp.float32),
        ),
        "kv",
    )
    projected = [(mix_factor * piece).astype(jnp.bfloat16) for piece in summed]
    query_one = projected[0].reshape(batch_rows, heads_here, head_dim)
    query_two = projected[1].reshape(batch_rows, heads_here, head_dim)
    key_one = projected[2].reshape(batch_rows, heads_here, head_dim)
    key_two = projected[3].reshape(batch_rows, heads_here, head_dim)
    new_value = projected[4].reshape(batch_rows, heads_here, 2 * head_dim)
    stats_one = block_softmax(query_one, key_cache[..., :head_dim], value_cache, head_dim)
    stats_two = block_softmax(query_two, key_cache[..., head_dim:], value_cache, head_dim)
    merged = merged_2(
        (stats_one[0], stats_one[1], stats_one[2], stats_two[0], stats_two[1], stats_two[2]),
        "kv",
        combine_maps,
    )
    own_one = jnp.einsum(
        "bhd,bhd->bh", query_one, key_one, preferred_element_type=jnp.float32
    ) * head_dim ** (-0.5)
    own_two = jnp.einsum(
        "bhd,bhd->bh", query_two, key_two, preferred_element_type=jnp.float32
    ) * head_dim ** (-0.5)
    attended = with_own(merged[0:3], own_one, new_value) - mix_lambda[:, None] * with_own(
        merged[3:6], own_two, new_value
    )
    head_factor = lax.rsqrt(jnp.mean(attended * attended, axis=-1, keepdims=True) + norm_eps)
    headed = (
        (attended * head_factor * head_gain)
        .astype(jnp.bfloat16)
        .reshape(batch_rows, heads_here * 2 * head_dim)
    )
    projection = summed_on_arrival(
        jnp.dot(headed, out_weight, preferred_element_type=jnp.float32).astype(jnp.bfloat16), TP, 1
    ).astype(jnp.bfloat16)
    second_own = (stream_own.astype(jnp.float32) + projection.astype(jnp.float32)).astype(
        jnp.bfloat16
    )
    second_whole = gather_axes(second_own, KV_TP, (1, 0, 2), 1)
    hidden_two = hidden_units(second_whole, gain_last, gate_last, up_last)
    mixed_last = sum_by_axis(down_term(hidden_two, down_last), KV_TP, (2, 0, 1), 0)
    return (second_own.astype(jnp.float32) + 0.5 * mixed_last.T).astype(jnp.bfloat16)


def solution(mesh):
    finer = Mesh(
        mesh.devices.reshape(mesh.shape["grp"], mesh.shape["kv"], 4, 2),
        ("grp", "kv", "tp_0", "tp_1"),
    )
    in_specs = (
        P("grp", KV_TP),
        P("grp", "kv", TP, None),
        P("grp", "kv", TP, None),
        P(),
        P(None, KV_TP),
        P(None, KV_TP),
        P(KV_TP, None),
        P(),
        P("kv", TP),
        P("kv", TP),
        P("kv", TP),
        P("kv", TP),
        P("kv", TP),
        P(TP),
        P(TP, None),
        P(TP, "kv"),
        P(),
        P(None, KV_TP),
        P(None, KV_TP),
        P(KV_TP, None),
    )
    out_specs = P("grp", KV_TP)
    return jax.shard_map(local, mesh=finer, in_specs=in_specs, out_specs=out_specs, check_vma=False)
```

profile of v0, /device:TPU:40, one launch (start us, length us, event | category | flops | bytes accessed | tf_op | source)
XLA Modules:
  0.0 454.0 jit_solution(2013131426868079877)
XLA Ops:
  6.6 11.7 %all-gather = bf16[32,32]{1,0:T(8,128)(2,1)S(1)} all-gather(bf16[8,32]{1,0:T(8,128)(2,1)} %param.20), channel_id=2, replica_groups=mesh['grp'=2,'kv'=16,'tp_0'=4,'tp_1'=2] {'tp_0'}, dimensions={0}, use_global_device_ids=true | all-gather | bytes 2560 | tf_op jit(solution)/shard_map/all_gather | solution.py:23
  18.3 49.0 %all-gather.1 = bf16[64,8,32]{2,1,0:T(8,128)(2,1)S(1)} all-gather(bf16[4,8,32]{2,1,0:T(8,128)(2,1)S(1)} %bitcast.237), channel_id=3, replica_groups=mesh['grp'=2,'kv'=16,'tp_0'=4,'tp_1'=2] {'kv'}, dimensions={0}, use_global_device_ids=true | all-gather | bytes 34816 | tf_op jit(solution)/shard_map/all_gather | solution.py:23
  67.2 2.1 all-gather.2
  69.4 0.2 fusion.18
  69.9 0.2 reshape.395
  70.1 0.3 convolution_multiply_fusion.3
  70.4 2.0 convolution_bitcast_fusion.1
  72.5 0.5 reshape_reshape.12
  72.9 1.1 copy.155
  74.2 8.2 %reduce-scatter.5.cloned.1.call-done = f32[64,32,8]{1,2,0:T(8,128)} async-done(((f32[128,32,8]{1,2,0:T(8,128)}), f32[64,32,8]{1,2,0:T(8,128)}) %reduce-scatter.5.cloned.1.call-update) | async-done | bytes 65552 | tf_op jit(solution)/shard_map/reduce_scatter | solution.py:40
  82.4 0.6 dynamic-slice
  83.1 0.8 dynamic_slice.7
  83.8 70.2 %reduce-scatter.7.cloned.1.call-done = f32[4,32,8]{1,2,0:T(8,128)} async-done(((f32[64,32,8]{1,2,0:T(8,128)}), f32[4,32,8]{1,2,0:T(8,128)}) %reduce-scatter.7.cloned.1.call-update) | async-done | bytes 4112 | tf_op jit(solution)/shard_map/reduce_scatter | solution.py:40
  154.1 17.5 %all-reduce.4 = f32[4,32,8]{1,2,0:T(8,128)S(1)} all-reduce(f32[4,32,8]{1,2,0:T(8,128)} %reduce-scatter.7.cloned.1.call-done), channel_id=13, replica_groups=mesh['grp'=2,'kv'=16,'tp_0'=4,'tp_1'=2] {'tp_0'}, use_global_device_ids=true, to_apply=%region_3.4.clone | all-reduce | flops 1024 | bytes 8192
  171.6 0.6 fusion.52
  172.2 10.5 %all-gather.3 = bf16[32,32]{1,0:T(8,128)(2,1)S(1)} all-gather(bf16[8,32]{1,0:T(8,128)(2,1)S(1)} %fusion.52), channel_id=5, replica_groups=mesh['grp'=2,'kv'=16,'tp_0'=4,'tp_1'=2] {'tp_0'}, dimensions={0}, use_global_device_ids=true | all-gather | bytes 2560 | tf_op jit(solution)/shard_map/all_gather | solution.py:23
  182.7 28.1 %all-gather.4 = bf16[64,8,32]{2,1,0:T(8,128)(2,1)S(1)} all-gather(bf16[4,8,32]{2,1,0:T(8,128)(2,1)S(1)} %bitcast.238), channel_id=6, replica_groups=mesh['grp'=2,'kv'=16,'tp_0'=4,'tp_1'=2] {'kv'}, dimensions={0}, use_global_device_ids=true | all-gather | bytes 34816 | tf_op jit(solution)/shard_map/all_gather | solution.py:23
  210.8 2.1 all-gather.5
  213.2 0.2 reshape.396
  214.1 1.0 broadcast_in_dim.4
  215.1 10.2 %all-to-all-start = ((f32[16,1,6144]{2,1,0:T(1,128)}), f32[16,1,6144]{2,1,0:T(1,128)S(1)}, u32[]{:S(2)}, u32[]{:S(2)}) async-start(f32[16,1,6144]{2,1,0:T(1,128)} %broadcast_in_dim.4), calls=%async_computation.2 | async-start | bytes 786432 | tf_op jit(solution)/shard_map/all_to_all | solution.py:56
  225.3 0.2 fusion.19
  225.5 23.8 %all-to-all-done = f32[16,1,6144]{2,1,0:T(1,128)S(1)} async-done(((f32[16,1,6144]{2,1,0:T(1,128)}), f32[16,1,6144]{2,1,0:T(1,128)S(1)}, u32[]{:S(2)}, u32[]{:S(2)}) %all-to-all-start) | async-done | bytes 393248 | tf_op jit(solution)/shard_map/all_to_all | solution.py:56
  249.3 0.2 reduce_sum.77
  249.8 1.6 fusion.12
  251.7 1.6 fusion.14
  253.7 0.4 fusion
  254.0 0.4 fusion.2
  254.5 0.8 broadcast_in_dim.5
  255.2 6.0 %all-to-all-start.1 = ((f32[16,20,256]{2,1,0:T(8,128)}), f32[16,20,256]{2,1,0:T(8,128)S(1)}, u32[]{:S(2)}, u32[]{:S(2)}) async-start(f32[16,20,256]{2,1,0:T(8,128)} %broadcast_in_dim.5), calls=%async_computation.3 | async-start | bytes 786432 | tf_op jit(solution)/shard_map/all_to_all | solution.py:56
  262.0 23.2 %all-to-all-done.1 = f32[16,20,256]{2,1,0:T(8,128)S(1)} async-done(((f32[16,20,256]{2,1,0:T(8,128)}), f32[16,20,256]{2,1,0:T(8,128)S(1)}, u32[]{:S(2)}, u32[]{:S(2)}) %all-to-all-start.1) | async-done | bytes 327712 | tf_op jit(solution)/shard_map/all_to_all | solution.py:56
  288.6 0.2 fusion.73
  288.8 0.2 fusion.75
  289.5 0.2 multiply_reduce_fusion
  290.1 8.8 %all_to_all.16 = bf16[8,2,128]{2,1,0:T(2,128)(2,1)S(1)} all-to-all(bf16[8,2,128]{2,1,0:T(2,128)(2,1)S(1)} %reshape.438), channel_id=1, replica_groups=mesh['grp'=2,'kv'=16,'tp_0'=4,'tp_1'=2] {'tp_0','tp_1'}, dimensions={0} | all-to-all | bytes 8192 | tf_op jit(solution)/shard_map/all_to_all | solution.py:106
  299.1 10.5 %all-gather.6 = bf16[32,32]{1,0:T(8,128)(2,1)S(1)} all-gather(bf16[8,32]{1,0:T(8,128)(2,1)S(1)} %add_convert_fusion), channel_id=8, replica_groups=mesh['grp'=2,'kv'=16,'tp_0'=4,'tp_1'=2] {'tp_0'}, dimensions={0}, use_global_device_ids=true | all-gather | bytes 2560 | tf_op jit(solution)/shard_map/all_gather | solution.py:23
  309.6 30.4 %all-gather.7 = bf16[64,8,32]{2,1,0:T(8,128)(2,1)S(1)} all-gather(bf16[4,8,32]{2,1,0:T(8,128)(2,1)S(1)} %bitcast.239), channel_id=9, replica_groups=mesh['grp'=2,'kv'=16,'tp_0'=4,'tp_1'=2] {'kv'}, dimensions={0}, use_global_device_ids=true | all-gather | bytes 34816 | tf_op jit(solution)/shard_map/all_gather | solution.py:23
  339.9 2.3 all-gather.8
  342.3 0.2 fusion.20
  342.7 0.2 reshape.397
  343.0 0.3 convolution_multiply_fusion.1
  343.3 2.0 convolution_bitcast_fusion
  345.3 0.5 reshape_reshape.15
  345.8 1.1 copy.178
  347.0 10.2 %reduce-scatter.9.cloned.1.call-done = f32[64,32,8]{1,2,0:T(8,128)} async-done(((f32[128,32,8]{1,2,0:T(8,128)}), f32[64,32,8]{1,2,0:T(8,128)}) %reduce-scatter.9.cloned.1.call-update) | async-done | bytes 65552 | tf_op jit(solution)/shard_map/reduce_scatter | solution.py:40
  357.2 71.6 %reduce-scatter.11.cloned.1.call-done = f32[4,32,8]{1,2,0:T(8,128)} async-done(((f32[64,32,8]{1,2,0:T(8,128)}), f32[4,32,8]{1,2,0:T(8,128)}) %reduce-scatter.11.cloned.1.call-update) | async-done | bytes 4112 | tf_op jit(solution)/shard_map/reduce_scatter | solution.py:40
  428.8 17.5 %all-reduce.5 = f32[4,32,8]{1,2,0:T(8,128)S(1)} all-reduce(f32[4,32,8]{1,2,0:T(8,128)} %reduce-scatter.11.cloned.1.call-done), channel_id=16, replica_groups=mesh['grp'=2,'kv'=16,'tp_0'=4,'tp_1'=2] {'tp_0'}, use_global_device_ids=true, to_apply=%region_15.16.clone | all-reduce | flops 1024 | bytes 8192
  446.2 1.2 fusion.51
  (135 shorter events, 6.9 us)
Async XLA Ops:
  6.5 247.1 %copy-start = (bf16[8,512,1,256]{3,1,2,0:T(8,128)(2,1)S(1)}, bf16[8,512,1,256]{3,1,2,0:T(8,128)(2,1)}, u32[]{:S(2)}) copy-start(bf16[8,512,1,256]{3,1,2,0:T(8,128)(2,1)} %param.22) | copy-start | bytes 6291460
  6.6 75.8 %reduce-scatter.5.cloned.1.call-start = ((), (), s32[]{:S(2)}) async-start(), calls=%async_computation.7 | async-start | bytes 786432 | tf_op jit(solution)/shard_map/reduce_scatter | solution.py:40
  67.2 2.9 copy-start.1
  67.2 2.9 copy-start.4
  70.4 12.0 %copy-start.13 = (u32[256]{0:T(256)S(1)}, u32[256]{0:T(256)}, u32[]{:S(2)}) copy-start(u32[256]{0:T(256)} %constant.62) | copy-start | bytes 3076
  70.4 101.2 %copy-start.10 = (bf16[8,32]{1,0:T(8,128)(2,1)S(1)}, bf16[8,32]{1,0:T(8,128)(2,1)}, u32[]{:S(2)}) copy-start(bf16[8,32]{1,0:T(8,128)(2,1)} %param.20) | copy-start | bytes 1540
  74.1 80.0 %reduce-scatter.7.cloned.1.call-start = ((), (), s32[]{:S(2)}) async-start(), calls=%async_computation.8 | async-start | bytes 278528 | tf_op jit(solution)/shard_map/reduce_scatter | solution.py:40
  82.4 131.0 %copy-start.3 = (bf16[256,256]{1,0:T(8,128)(2,1)S(1)}, bf16[256,256]{1,0:T(8,128)(2,1)}, u32[]{:S(2)}) copy-start(bf16[256,256]{1,0:T(8,128)(2,1)} %param.32) | copy-start | bytes 393220
  182.7 30.8 %copy-start.6 = (bf16[256,128]{1,0:T(8,128)(2,1)S(1)}, bf16[256,128]{1,0:T(8,128)(2,1)}, u32[]{:S(2)}) copy-start(bf16[256,128]{1,0:T(8,128)(2,1)} %param.28) | copy-start | bytes 196612
  210.8 2.9 copy-start.7
  210.8 3.0 copy-start.8
  210.8 3.2 copy-start.9
  215.1 34.3 %all-to-all-start = ((f32[16,1,6144]{2,1,0:T(1,128)}), f32[16,1,6144]{2,1,0:T(1,128)S(1)}, u32[]{:S(2)}, u32[]{:S(2)}) async-start(f32[16,1,6144]{2,1,0:T(1,128)} %broadcast_in_dim.4), calls=%async_computation.2 | async-start | bytes 786432 | tf_op jit(solution)/shard_map/all_to_all | solution.py:56
  254.4 35.3 %copy-start.11 = (bf16[256,256]{1,0:T(8,128)(2,1)S(1)}, bf16[256,256]{1,0:T(8,128)(2,1)}, u32[]{:S(2)}) copy-start(bf16[256,256]{1,0:T(8,128)(2,1)} %param.35) | copy-start | bytes 393220
  254.4 35.3 %copy-start.12 = (f32[1,256]{1,0:T(1,128)S(1)}, f32[1,256]{1,0:T(1,128)}, u32[]{:S(2)}) copy-start(f32[1,256]{1,0:T(1,128)} %param.34) | copy-start | bytes 3076
  255.2 29.9 %all-to-all-start.1 = ((f32[16,20,256]{2,1,0:T(8,128)}), f32[16,20,256]{2,1,0:T(8,128)S(1)}, u32[]{:S(2)}, u32[]{:S(2)}) async-start(f32[16,20,256]{2,1,0:T(8,128)} %broadcast_in_dim.5), calls=%async_computation.3 | async-start | bytes 786432 | tf_op jit(solution)/shard_map/all_to_all | solution.py:56
  261.3 95.9 %reduce-scatter.9.cloned.1.call-start = ((), (), s32[]{:S(2)}) async-start(), calls=%async_computation.9 | async-start | bytes 786432 | tf_op jit(solution)/shard_map/reduce_scatter | solution.py:40
  339.9 3.1 copy-start.2
  339.9 3.1 copy-start.5
  346.9 81.9 %reduce-scatter.11.cloned.1.call-start = ((), (), s32[]{:S(2)}) async-start(), calls=%async_computation.10 | async-start | bytes 278528 | tf_op jit(solution)/shard_map/reduce_scatter | solution.py:40
Sparse Core Ops, SparseCore 0:
  74.2 8.0 reduce-scatter.4
  84.9 69.1 reduce-scatter.6
  347.0 10.0 reduce-scatter.8
  359.5 69.2 reduce-scatter.10
where the time goes:
time: 455 us; the launch traced here: 454 us
  waiting for transfers between devices  207 us (45%)
  blocking collectives  191 us (42%)
  starting transfers between devices  16.4 us (4%)
  between operations  14.3 us (3%)
  local copies, waits for them, and re-layouts  11 us (2%)
  matrix products  9.43 us (2%)
  other arithmetic  5.03 us (1%)
    reduce_scatter x4, waiting for transfers between devices, reduced_to_own(): pieces = lax.psum_scatter(pieces, axes[k], scatter_dimension=0, tiled=True)  160 us
    all_gather x9, blocking collectives, gather_in_order(): pieces = lax.all_gather(pieces, axes[k])  147 us
    all_to_all x2, waiting for transfers between devices, copy_for_each(): lax.all_to_all(jnp.broadcast_to(shard[None], (count, *shard.shape)), axis...  47 us
    unnamed x2, blocking collectives  35 us
    all_to_all x2, starting transfers between devices, copy_for_each(): lax.all_to_all(jnp.broadcast_to(shard[None], (count, *shard.shape)), axis...  16.2 us
  transfers between devices with their start and end apart: 6, of which 6 were waited for; matrix products, arithmetic and copies ran while one was open for 0% of the time, Pallas kernels for 0%

commit v1 on v0

v1 whole, which is shorter than its diff:
```python
import functools

import jax
import jax.numpy as jnp
from jax import lax
from jax.experimental import pallas as pl
from jax.experimental.pallas import tpu as pltpu
from jax.sharding import PartitionSpec as P

MESH = pl.DeviceIdType.MESH
F32 = jnp.float32
BF16 = jnp.bfloat16
norm_eps = 1e-06
LOW = -1e30
LANES = 128

PHASES = 13
(A_TP, A_KV, B_TP, B_KV, D_Q, D_ROW, D_SQ, E_ACC, E_STAT, F_TP, G_KV, H_TP, H_KV) = range(PHASES)


def nt(a, b):
    return lax.dot_general(a, b, (((1,), (1,)), ((), ())), preferred_element_type=F32)


def nn(a, b):
    return lax.dot_general(a, b, (((1,), (0,)), ((), ())), preferred_element_type=F32)


def outward(n):
    return sorted(range(1, n), key=lambda k: (-min(k, n - k), k))


def layer_kernel(
    n_kv,
    n_tp,
    tokens,
    key_cache,
    value_cache,
    gain_first,
    gate_first,
    up_first,
    down_first,
    gain_mix,
    query_first,
    query_second,
    key_first,
    key_second,
    value_weight,
    mix_lambda,
    head_gain,
    out_weight,
    gain_last,
    gate_last,
    up_last,
    down_last,
    out_ref,
    tok_v,
    key_v,
    value_v,
    gains_v,
    gate_v,
    up_v,
    down_v,
    proj_v,
    lam_v,
    head_gain_v,
    out_v,
    a_tp,
    a_kv,
    g_kv,
    b_out,
    b_in,
    b_tp,
    h_out,
    h_in,
    h_half,
    h_tp,
    d_q,
    d_rows32,
    d_rows,
    d_rowr,
    d_sq,
    e_acc,
    e_stat,
    f_tp,
    load_sem,
    send_sem,
    recv_sem,
):
    kv = lax.axis_index("kv")
    tp = lax.axis_index("tp")
    rows, own = tokens.shape
    per_tile = LANES // own
    plane = own * n_tp
    width = plane * n_kv
    head_dim = query_first.shape[1]
    sizes = {"kv": n_kv, "tp": n_tp}
    here = {"kv": kv, "tp": tp}

    barrier = pltpu.get_barrier_semaphore()
    for axis in ("kv", "tp"):
        for k in range(1, sizes[axis]):
            peer = lax.rem(here[axis] + k, sizes[axis])
            pl.semaphore_signal(barrier, inc=1, device_id={axis: peer}, device_id_type=MESH)

    loads = []

    def load(src, dst):
        copy = pltpu.make_async_copy(src, dst, load_sem.at[len(loads)])
        copy.start()
        loads.append(copy)
        return copy

    load_tok = load(tokens, tok_v)
    load_first = [
        load(gain_first, gains_v.at[0]),
        load(gate_first, gate_v.at[0]),
        load(up_first, up_v.at[0]),
        load(down_first, down_v.at[0]),
    ]
    load_proj = [load(gain_mix, gains_v.at[1])]
    at = 0
    for weight in (query_first, query_second, key_first, key_second, value_weight):
        load_proj.append(load(weight, proj_v.at[:, pl.ds(at, weight.shape[1])]))
        at += weight.shape[1]
    load_cache = [load(key_cache, key_v), load(value_cache, value_v)]
    load_out = [load(mix_lambda, lam_v), load(head_gain, head_gain_v), load(out_weight, out_v)]
    load_last = [
        load(gain_last, gains_v.at[2]),
        load(gate_last, gate_v.at[1]),
        load(up_last, up_v.at[1]),
        load(down_last, down_v.at[1]),
    ]

    pl.semaphore_wait(barrier, n_kv + n_tp - 2)

    sends = []

    def send(axis, phase, k, src, dst):
        copy = pltpu.make_async_remote_copy(
            src_ref=src,
            dst_ref=dst.at[here[axis]],
            send_sem=send_sem.at[phase, k],
            recv_sem=recv_sem.at[phase, k],
            device_id={axis: lax.rem(here[axis] + k, sizes[axis])},
            device_id_type=MESH,
        )
        copy.start()
        sends.append(copy)

    def send_all(axis, phase, src_of, dst):
        for k in outward(sizes[axis]):
            send(axis, phase, k, src_of(lax.rem(here[axis] + k, sizes[axis])), dst)

    def arrived(axis, phase, dst, k):
        peer = lax.rem(here[axis] - k + sizes[axis], sizes[axis])
        pltpu.make_async_remote_copy(
            src_ref=dst.at[peer],
            dst_ref=dst.at[peer],
            send_sem=send_sem.at[phase, k],
            recv_sem=recv_sem.at[phase, k],
            device_id={axis: peer},
            device_id_type=MESH,
        ).wait_recv()
        return peer

    def all_arrived(axis, phase, dst):
        for k in reversed(outward(sizes[axis])):
            arrived(axis, phase, dst, k)

    lane = lax.broadcasted_iota(jnp.int32, (rows, LANES), 1)
    tile_place = lax.rem(tp, per_tile)
    tile_half = tp // per_tile

    def tp_gather(tile, phase, buf):
        buf[tp] = tile.astype(BF16)
        send_all("tp", phase, lambda peer: buf.at[tp], buf)
        all_arrived("tp", phase, buf)
        halves = []
        for first in range(0, n_tp, per_tile):
            total = buf[first].astype(F32)
            for t in range(first + 1, first + per_tile):
                total += buf[t].astype(F32)
            halves.append(total)
        return jnp.concatenate(halves, axis=1)

    def block_hidden(buf, phase, which):
        gate = jnp.zeros((rows, gate_v.shape[1]), F32)
        up = jnp.zeros((rows, up_v.shape[1]), F32)
        square = jnp.zeros((rows, 1), F32)
        for k in [0] + outward(n_kv)[::-1]:
            peer = kv if k == 0 else arrived("kv", phase, buf, k)
            columns = pl.ds(pl.multiple_of(peer * plane, plane), plane)
            wide = buf[peer].astype(F32)
            square += jnp.sum(wide * wide, axis=1, keepdims=True)
            normed = (wide * gains_v[which, :, columns]).astype(BF16)
            slot = 0 if which == 0 else 1
            gate += nt(normed, gate_v[slot, :, columns])
            up += nt(normed, up_v[slot, :, columns])
        factor = lax.rsqrt(square / width + norm_eps)
        gate, up = factor * gate, factor * up
        return (gate / (1.0 + jnp.exp(-gate)) * up).astype(BF16)

    def sum_over_kv(hidden, slot, phase, out_buf, in_buf):
        for k in outward(n_kv) + [0]:
            peer = lax.rem(kv + k, n_kv)
            columns = pl.ds(pl.multiple_of(peer * plane, plane), plane)
            part = nn(hidden, down_v[slot, :, columns]).astype(BF16)
            if k == 0:
                in_buf[kv] = part
            else:
                out_buf[k] = part
                send("kv", phase, k, out_buf.at[k], in_buf)
        all_arrived("kv", phase, in_buf)
        total = in_buf[0].astype(F32)
        for p in range(1, n_kv):
            total += in_buf[p].astype(F32)
        return total

    def sum_over_tp(phase, buf):
        all_arrived("tp", phase, buf)
        total = buf[0].astype(F32)
        for t in range(1, n_tp):
            total += buf[t].astype(F32)
        return total

    def wait(copies):
        for copy in copies:
            copy.wait()

    load_tok.wait()
    pick = lax.broadcasted_iota(jnp.int32, (own, LANES), 1) == (
        lax.broadcasted_iota(jnp.int32, (own, LANES), 0) + tile_place * own
    )
    tok_tile = nn(tok_v[...], pick.astype(F32).astype(BF16))
    tok_plane = tp_gather(tok_tile, A_TP, a_tp)
    a_kv[kv] = tok_plane.astype(BF16)
    send_all("kv", A_KV, lambda peer: a_kv.at[kv], a_kv)
    wait(load_first)
    hidden = block_hidden(a_kv, A_KV, 0)

    b_tp[tp] = sum_over_kv(hidden, 0, B_KV, b_out, b_in).astype(BF16)
    send_all("tp", B_TP, lambda peer: b_tp.at[tp], b_tp)
    first = (tok_plane + 0.5 * sum_over_tp(B_TP, b_tp)).astype(BF16).astype(F32)

    wait(load_proj)
    my_columns = pl.ds(pl.multiple_of(kv * plane, plane), plane)
    normed = (first * gains_v[1, :, my_columns]).astype(BF16)
    pair = 2 * head_dim
    d_q[kv] = nn(normed, proj_v[:, 0:pair]).astype(BF16)
    send_all("kv", D_Q, lambda peer: d_q.at[kv], d_q)
    square = jnp.sum(first * first, axis=1, keepdims=True)
    row_of = lax.broadcasted_iota(jnp.int32, (rows, LANES), 0)
    d_sq[kv] = jnp.sum(jnp.where(lane == row_of, square, 0.0), axis=0, keepdims=True)
    send_all("kv", D_SQ, lambda peer: d_sq.at[kv], d_sq)
    others = nn(normed, proj_v[:, pair:])
    groups = others.shape[1] // LANES
    for g in range(groups):
        d_rows32[pl.ds(g, rows, stride=groups), :] = others[:, g * LANES : (g + 1) * LANES]
    for b in range(rows):
        d_rows[b] = d_rows32[b * groups : (b + 1) * groups, :].astype(BF16)
    homes = n_kv // rows
    send_all("kv", D_ROW, lambda peer: d_rows.at[peer // homes], d_rowr)
    d_rowr[kv] = d_rows[kv // homes]

    all_arrived("kv", D_SQ, d_sq)
    square_row = d_sq[0]
    for p in range(1, n_kv):
        square_row += d_sq[p]
    square = jnp.sum(
        jnp.where(lane == row_of, jnp.broadcast_to(square_row, (rows, LANES)), 0.0), axis=1, keepdims=True
    )
    factor = lax.rsqrt(square / width + norm_eps)
    all_arrived("kv", D_Q, d_q)
    query = d_q[0].astype(F32)
    for p in range(1, n_kv):
        query += d_q[p].astype(F32)
    query = (factor * query).astype(BF16).astype(F32)

    wait(load_cache)
    both = 2 * rows
    scale = head_dim ** (-0.5)
    zero = jnp.zeros((rows, head_dim), F32)
    stacked = jnp.concatenate(
        [
            jnp.concatenate([query[:, :head_dim], zero], axis=1),
            jnp.concatenate([zero, query[:, head_dim:]], axis=1),
        ],
        axis=0,
    )
    sequence = lax.rem(lax.broadcasted_iota(jnp.int32, (both, 1), 0), rows)
    scores = None
    for b in range(rows):
        term = nt(jnp.where(sequence == b, stacked, 0.0).astype(BF16), key_v[b])
        scores = term if scores is None else scores + term
    scores = scores * scale
    top = jnp.max(scores, axis=1, keepdims=True)
    weights = jnp.exp(scores - top)
    weight_sum = jnp.sum(weights, axis=1, keepdims=True)
    weighted = None
    for b in range(rows):
        term = nn(jnp.where(sequence == b, weights, 0.0).astype(BF16), value_v[b])
        weighted = term if weighted is None else weighted + term

    all_arrived("kv", D_ROW, d_rowr)
    own_rows = d_rowr[0].astype(F32)
    for p in range(1, n_kv):
        own_rows += d_rowr[p].astype(F32)
    my_row = kv // homes
    is_mine = sequence == my_row
    own_factor = jnp.sum(
        jnp.where(lax.broadcasted_iota(jnp.int32, (rows, 1), 0) == my_row, factor, 0.0), axis=0, keepdims=True
    )
    own_rows = (own_factor * own_rows).astype(BF16).astype(F32)
    own_keys = jnp.concatenate([own_rows[0:1], own_rows[1:2]], axis=1)
    own_value = jnp.concatenate([own_rows[2:3], own_rows[3:4]], axis=1)
    own_score = jnp.sum(stacked * own_keys, axis=1, keepdims=True) * scale
    is_home = jnp.logical_and(is_mine, lax.rem(kv, homes) == 0)
    own_score = jnp.where(is_home, own_score, LOW)
    new_top = jnp.maximum(top, own_score)
    old_factor = jnp.exp(top - new_top)
    own_weight = jnp.where(is_home, jnp.exp(own_score - new_top), 0.0)
    weight_sum = old_factor * weight_sum + own_weight
    weighted = old_factor * weighted + own_weight * own_value
    top = new_top

    wide_lane = lax.broadcasted_iota(jnp.int32, (both, LANES), 1)
    wide_row = lax.broadcasted_iota(jnp.int32, (both, LANES), 0)
    diagonal = wide_lane == wide_row
    as_row = lambda column: jnp.sum(jnp.where(diagonal, column, 0.0), axis=0, keepdims=True)
    as_column = lambda row: jnp.sum(
        jnp.where(diagonal, jnp.broadcast_to(row, (both, LANES)), 0.0), axis=1, keepdims=True
    )
    e_acc[kv] = weighted.astype(BF16)
    e_stat[kv] = jnp.concatenate([as_row(top), as_row(weight_sum)], axis=0)
    send_all("kv", E_STAT, lambda peer: e_stat.at[kv], e_stat)
    send_all("kv", E_ACC, lambda peer: e_acc.at[kv], e_acc)
    all_arrived("kv", E_STAT, e_stat)
    stats = [e_stat[p] for p in range(n_kv)]
    top_row = functools.reduce(jnp.maximum, [s[0:1] for s in stats])
    shares = [jnp.exp(s[0:1] - top_row) for s in stats]
    total_row = functools.reduce(jnp.add, [f * s[1:2] for f, s in zip(shares, stats)])
    columns = [as_column(f) for f in shares]
    total = as_column(total_row)
    all_arrived("kv", E_ACC, e_acc)
    merged = functools.reduce(jnp.add, [c * e_acc[p].astype(F32) for p, c in enumerate(columns)])
    merged = merged / total
    wait(load_out)
    attended = merged[:rows] - lam_v[...] * merged[rows:]
    head_factor = lax.rsqrt(jnp.mean(attended * attended, axis=1, keepdims=True) + norm_eps)
    headed = (attended * head_factor * head_gain_v[...]).astype(BF16)

    f_tp[tp] = nn(headed, out_v[...]).astype(BF16)
    send_all("tp", F_TP, lambda peer: f_tp.at[tp], f_tp)
    projection = sum_over_tp(F_TP, f_tp)
    second = (first + projection.astype(BF16).astype(F32)).astype(BF16)

    g_kv[kv] = second
    send_all("kv", G_KV, lambda peer: g_kv.at[kv], g_kv)
    wait(load_last)
    hidden = block_hidden(g_kv, G_KV, 2)
    summed = sum_over_kv(hidden, 1, H_KV, h_out, h_in).astype(BF16)
    second = second.astype(F32)
    second_tile = jnp.zeros((rows, LANES), F32)
    for half in range(n_tp // per_tile):
        tile = slice(half * LANES, (half + 1) * LANES)
        h_half[half] = summed[:, tile]
        second_tile = jnp.where(tile_half == half, second[:, tile], second_tile)
    send_all("tp", H_TP, lambda peer: h_half.at[peer // per_tile], h_tp)
    h_tp[tp] = h_half[tile_half]
    updated = second_tile + 0.5 * sum_over_tp(H_TP, h_tp)
    turn = lax.rem(per_tile - tile_place, per_tile) * own
    out_ref[...] = pltpu.roll(updated, turn, 1)[:, :own].astype(BF16)
    for copy in sends:
        copy.wait_send()


def solution(mesh):
    n_kv, n_tp = mesh.shape["kv"], mesh.shape["tp"]
    both_axes = ("kv", "tp")

    def step(*args):
        (
            tokens,
            key_cache,
            value_cache,
            gain_first,
            gate_first,
            up_first,
            down_first,
            gain_mix,
            query_first,
            query_second,
            key_first,
            key_second,
            value_weight,
            mix_lambda,
            head_gain,
            out_weight,
            gain_last,
            gate_last,
            up_last,
            down_last,
        ) = args
        rows, own = tokens.shape
        plane = own * n_tp
        width = plane * n_kv
        hidden = gate_first.shape[1]
        positions, head_width = key_cache.shape[1], key_cache.shape[3]
        proj_width = 2 * query_first.shape[1] + 2 * key_first.shape[1] + value_weight.shape[1]
        groups = (proj_width - 2 * query_first.shape[1]) // LANES
        cache_shape = (rows, positions, head_width)
        operands = (
            tokens,
            key_cache.reshape(cache_shape),
            value_cache.reshape(cache_shape),
            gain_first.reshape(1, width),
            gate_first.T,
            up_first.T,
            down_first,
            gain_mix.reshape(1, width),
            query_first,
            query_second,
            key_first,
            key_second,
            value_weight,
            mix_lambda.reshape(1, 1),
            head_gain,
            out_weight,
            gain_last.reshape(1, width),
            gate_last.T,
            up_last.T,
            down_last,
        )
        scratch = [
            pltpu.VMEM((rows, own), BF16),
            pltpu.VMEM(cache_shape, BF16),
            pltpu.VMEM(cache_shape, BF16),
            pltpu.VMEM((3, 1, width), F32),
            pltpu.VMEM((2, hidden, width), BF16),
            pltpu.VMEM((2, hidden, width), BF16),
            pltpu.VMEM((2, hidden, width), BF16),
            pltpu.VMEM((plane, proj_width), BF16),
            pltpu.VMEM((1, 1), F32),
            pltpu.VMEM((1, head_width), F32),
            pltpu.VMEM(out_weight.shape, BF16),
            pltpu.VMEM((n_tp, rows, LANES), BF16),
            pltpu.VMEM((n_kv, rows, plane), BF16),
            pltpu.VMEM((n_kv, rows, plane), BF16),
            pltpu.VMEM((n_kv, rows, plane), BF16),
            pltpu.VMEM((n_kv, rows, plane), BF16),
            pltpu.VMEM((n_tp, rows, plane), BF16),
            pltpu.VMEM((n_kv, rows, plane), BF16),
            pltpu.VMEM((n_kv, rows, plane), BF16),
            pltpu.VMEM((plane // LANES, rows, LANES), BF16),
            pltpu.VMEM((n_tp, rows, LANES), BF16),
            pltpu.VMEM((n_kv, rows, 2 * query_first.shape[1]), BF16),
            pltpu.VMEM((rows * groups, LANES), F32),
            pltpu.VMEM((rows, groups, LANES), BF16),
            pltpu.VMEM((n_kv, groups, LANES), BF16),
            pltpu.VMEM((n_kv, 1, LANES), F32),
            pltpu.VMEM((n_kv, 2 * rows, head_width), BF16),
            pltpu.VMEM((n_kv, 2, LANES), F32),
            pltpu.VMEM((n_tp, rows, plane), BF16),
            pltpu.SemaphoreType.DMA((len(operands),)),
            pltpu.SemaphoreType.DMA((PHASES, max(n_kv, n_tp))),
            pltpu.SemaphoreType.DMA((PHASES, max(n_kv, n_tp))),
        ]
        return pl.pallas_call(
            functools.partial(layer_kernel, n_kv, n_tp),
            out_shape=jax.ShapeDtypeStruct((rows, own), BF16),
            in_specs=[pl.BlockSpec(memory_space=pl.ANY)] * len(operands),
            out_specs=pl.BlockSpec(memory_space=pltpu.VMEM),
            scratch_shapes=scratch,
            compiler_params=pltpu.CompilerParams(collective_id=0, has_side_effects=True),
            name="layer",
        )(*operands)

    in_specs = (
        P("grp", both_axes),
        P("grp", "kv", "tp", None),
        P("grp", "kv", "tp", None),
        P(),
        P(None, both_axes),
        P(None, both_axes),
        P(both_axes, None),
        P(),
        P("kv", "tp"),
        P("kv", "tp"),
        P("kv", "tp"),
        P("kv", "tp"),
        P("kv", "tp"),
        P("tp"),
        P("tp", None),
        P("tp", "kv"),
        P(),
        P(None, both_axes),
        P(None, both_axes),
        P(both_axes, None),
    )
    return jax.shard_map(step, mesh=mesh, in_specs=in_specs, out_specs=P("grp", both_axes), check_vma=False)
```

time: 455 us -> 98.6 us (0.22)
  waiting for transfers between devices: 207 us -> 0 us
  blocking collectives: 191 us -> 0 us
  Pallas kernels: 0 us -> 95.7 us
  starting transfers between devices: 16.4 us -> 0 us
  between operations: 14.3 us -> 0.66 us
  local copies, waits for them, and re-layouts: 11 us -> 1.26 us
  matrix products: 9.43 us -> 0 us
  other arithmetic: 5.03 us -> 0 us
    reduce_scatter x4 -> x0, waiting for transfers between devices: 160 us -> none  [reduced_to_own(): pieces = lax.psum_scatter(pieces, axes[k], scatter_dimension=0, tiled=True)]
    all_gather x9 -> x0, blocking collectives: 147 us -> none  [gather_in_order(): pieces = lax.all_gather(pieces, axes[k])]
    pallas_call x0 -> x1, Pallas kernels: none -> 95.7 us  [step(): pl.pallas_call(functools.partial(layer_kernel, n_kv, n_tp), out_shape=jax...]
    all_to_all x2 -> x0, waiting for transfers between devices: 47 us -> none  [copy_for_each(): lax.all_to_all(jnp.broadcast_to(shard[None], (count, *shard.shape)), axis...]
    unnamed x2 -> x0, blocking collectives: 35 us -> none
    all_to_all x2 -> x0, starting transfers between devices: 16.2 us -> none  [copy_for_each(): lax.all_to_all(jnp.broadcast_to(shard[None], (count, *shard.shape)), axis...]
    dot_general x14 -> x0, matrix products: 9.43 us -> none  [the longest x2 4.06 us: down_term(): lax.dot_general(weight_down, hidden, (((0,), (1,)), ((), ())), preferred_...]
    all_to_all x1 -> x0, blocking collectives: 8.81 us -> none  [summed_on_arrival(): lax.all_to_all(pieces, axis, split_axis=0, concat_axis=0, tiled=True)]
  transfers between devices with their start and end apart: 6 -> 0, of which waited for: 6 -> 0; matrix products, arithmetic and copies ran while one was open for 0% -> 0% of each run, Pallas kernels for 0% -> 0%
where the time goes in v1:
time: 98.6 us; the launch traced here: 97.6 us
  Pallas kernels  95.7 us (97%)
  local copies, waits for them, and re-layouts  1.26 us (1%)
    pallas_call x1, Pallas kernels, step(): pl.pallas_call(functools.partial(layer_kernel, n_kv, n_tp), out_shape=jax...  95.7 us

profile of v1, /device:TPU:40, one launch (start us, length us, event | category | flops | bytes accessed | tf_op | source)
XLA Modules:
  0.0 97.6 jit_solution(1146324915857805311)
XLA Ops:
  0.7 95.7 %layer.1 = bf16[8,32]{1,0:T(8,128)(2,1)} custom-call(bf16[8,32]{1,0:T(8,128)(2,1)} %tokens.1, bf16[8,512,256]{2,1,0:T(8,128)(2,1)} %bitcast.11, bf16[8,512,256]{2,1,0:T(8,128)(2,1)} %bitcast.12, f32[1,4096]{1,0:T(1,128)} %bitcast.17, bf16[86,4096]{1,0:T(8,128)(2,1)} %bitcast.13, bf16[86,4096]{1,0:T(8,128)(2,1)} %bitcast.14, bf16[86,4096]{1,0:T(8,128)(2,1)} %down_first.1, ...), custom_call_target="tpu_custom_call" | custom-call | tf_op jit(solution)/shard_map/layer/pallas_call | solution.py:469
  96.3 1.3 %copy.23 = bf16[8,32]{1,0:T(8,128)(2,1)} copy(bf16[8,32]{1,0:T(8,128)(2,1)} %layer.1) | data formatting | bytes 1024
